TPU v7x, 32 devices: a whole 2x2x4 slice. The times are simulated.
32 devices in a mesh: ep: 16 (over z, y, x), tp: 2 (over core).
Axes of the slice: x: 2, y: 2, z: 4, core: 2. Of those that a mesh axis runs over, the one named last changes fastest.
Arguments:
- tokens: bfloat16 [8192, 2048], P(('ep', 'tp')), may hold values from -6 to 6
- norm_gain: float32 [2048], replicated, may hold values from 0.1 to 1.9
- expert_ids: int32 [8192, 2], P(('ep', 'tp')), may hold values from 0 to 15, all different within a row; in each aligned block of 256 rows (0 to 255, 256 to 511, ...) at most 48 rows name the same one
- route_weights: float32 [8192, 2], P(('ep', 'tp')), may hold values from 0.2 to 1.2
- expert_gate: bfloat16 [16, 2048, 512], P('ep', None, 'tp'), may hold values from -0.125 to 0.125
- expert_up: bfloat16 [16, 2048, 512], P('ep', None, 'tp'), may hold values from -0.125 to 0.125
- expert_down: bfloat16 [16, 512, 2048], P('ep', 'tp'), may hold values from -0.25 to 0.25
- shared_gate: bfloat16 [2048, 512], P(None, 'tp'), may hold values from -0.125 to 0.125
- shared_up: bfloat16 [2048, 512], P(None, 'tp'), may hold values from -0.125 to 0.125
- shared_down: bfloat16 [512, 2048], P('tp'), may hold values from -0.25 to 0.25
Outputs:
- mixed: bfloat16 [8192, 2048], P(('ep', 'tp'))
Inputs may be any that keep to these rules, and one draw needn't show every extreme that they name: `expert_ids`: each token names 2 different experts. Among the tokens of one device (aligned blocks of 256 rows) no expert is named by more than 48 tokens, and in every block some expert is named by exactly 48.
All inputs are finite; a program needn't handle non-finite values.
Results may differ from a plain program's by a relative error of at most 0.0075.
Values may be sent and summed in bfloat16 or wider, within the bound.
A program may use at most 64 MiB of HBM per device.

v0:
```python
import functools

import jax
import jax.numpy as jnp
from jax import lax
from jax.experimental import pallas as pl
from jax.experimental.pallas import tpu as pltpu
from jax.sharding import PartitionSpec as P

epsilon = 1e-06
MESH = pl.DeviceIdType.MESH


def toggled(index, step, size):
    total, bit = 0, 1
    while bit < size:
        total = total + bit * ((index // bit + step // bit) % 2)
        bit *= 2
    return total


def gated_sum(rows, gate_w, up_w, down_w):
    total = None
    for half in range(gate_w.shape[0]):
        gate_value = jnp.dot(rows, gate_w[half], preferred_element_type=jnp.float32)
        up_value = jnp.dot(rows, up_w[half], preferred_element_type=jnp.float32)
        hidden = (gate_value / (1.0 + jnp.exp(-gate_value)) * up_value).astype(jnp.bfloat16)
        term = jnp.dot(hidden, down_w[half], preferred_element_type=jnp.float32)
        total = term if total is None else total + term
    return total


def slot_rows(meta, me, steps):
    count = meta.shape[1]
    relative = meta[0:2, :].astype(jnp.int32) ^ me
    step_of = lax.broadcasted_iota(jnp.int32, (steps, count), 0)
    named = (step_of == relative[0:1, :]) | (step_of == relative[1:2, :])
    row_at = lax.broadcasted_iota(jnp.int32, (count, count), 0)
    col_at = lax.broadcasted_iota(jnp.int32, (count, count), 1)
    before = jnp.where(row_at < col_at, 1.0, 0.0).astype(jnp.bfloat16)
    slots = jnp.dot(
        jnp.where(named, 1.0, 0.0).astype(jnp.bfloat16), before, preferred_element_type=jnp.float32
    ).astype(jnp.int32)
    return jnp.where(named, slots, -1)


def picks(slots, steps, capacity):
    slot_at = lax.broadcasted_iota(jnp.int32, (capacity, slots.shape[1]), 0)
    return jnp.concatenate(
        [
            jnp.where(slot_at == slots[step : step + 1, :], 1.0, 0.0).astype(jnp.bfloat16)
            for step in steps
        ],
        axis=0,
    )


def slot_places(meta, me, capacity):
    count = meta.shape[1]
    turned = jnp.transpose(meta)
    relative = turned[:, 0:2].astype(jnp.int32) ^ me
    expert_at = lax.broadcasted_iota(jnp.int32, (count, 128), 1)
    row_at = lax.broadcasted_iota(jnp.int32, (count, count), 0)
    col_at = lax.broadcasted_iota(jnp.int32, (count, count), 1)
    chosen = [expert_at == relative[:, j : j + 1] for j in range(2)]
    after = jnp.where(row_at > col_at, 1.0, 0.0).astype(jnp.bfloat16)
    counted = jnp.dot(
        after,
        jnp.where(chosen[0] | chosen[1], 1.0, 0.0).astype(jnp.bfloat16),
        preferred_element_type=jnp.float32,
    )
    places = [
        relative[:, j : j + 1] * capacity
        + jnp.sum(jnp.where(chosen[j], counted, 0.0), axis=1, keepdims=True).astype(jnp.int32)
        for j in range(2)
    ]
    return places, [turned[:, 2 + j : 3 + j] for j in range(2)]


def weight_matrix(places, weights, first, amount):
    at = lax.broadcasted_iota(jnp.int32, (places[0].shape[0], amount), 1) + first
    scale = jnp.where(at == places[0], weights[0], 0.0) + jnp.where(
        at == places[1], weights[1], 0.0
    )
    upper = scale.astype(jnp.bfloat16)
    return upper, (scale - upper.astype(jnp.float32)).astype(jnp.bfloat16)


def weighted(pair, block):
    return jnp.dot(pair[0], block, preferred_element_type=jnp.float32) + jnp.dot(
        pair[1], block, preferred_element_type=jnp.float32
    )


def layer_kernel(
    peers,
    capacity,
    pieces,
    tokens,
    gain,
    meta,
    expert_gate,
    expert_up,
    expert_down,
    shared_gate,
    shared_up,
    shared_down,
    mixed,
    gate_all,
    up_all,
    down_all,
    s_gate_all,
    s_up_all,
    s_down_all,
    normed,
    cut,
    outgoing,
    received,
    results,
    returned,
    total,
    relay_in,
    meta_in,
    relay_out,
    relay_back,
    sums_out,
    sums_in,
    weight_local,
    weight_send,
    weight_recv,
    out_send,
    out_recv,
    back_send,
    back_recv,
    block_send,
    block_recv,
    meta_send,
    meta_recv,
    relay_send,
    relay_recv,
    home_send,
    home_recv,
    sums_send,
    sums_recv,
):
    me = lax.axis_index("ep")
    core = lax.axis_index("tp")
    sibling = 1 - core
    width = tokens.shape[1]
    piece = width // pieces
    half, quarter = peers // 2, peers // 4

    def is_inner(index):
        return ((index // quarter + 1) // 2) % 2

    inner = is_inner(me)
    turns = (half, half + quarter)

    def at_step(step):
        return (toggled(me, step, peers), core)

    def remote(source, target, send, recv, place):
        return pltpu.make_async_remote_copy(
            src_ref=source,
            dst_ref=target,
            send_sem=send,
            recv_sem=recv,
            device_id=place,
            device_id_type=MESH,
        )

    barrier = pltpu.get_barrier_semaphore()
    partners = range(1, peers)
    pl.semaphore_signal(barrier, inc=1, device_id=(me, sibling), device_id_type=MESH)
    for step in partners:
        pl.semaphore_signal(barrier, inc=1, device_id=at_step(step), device_id_type=MESH)
    sources = (
        (shared_gate, s_gate_all),
        (shared_up, s_up_all),
        (shared_down, s_down_all),
        (expert_gate, gate_all),
        (expert_up, up_all),
        (expert_down, down_all),
    )
    local = [
        pltpu.make_async_copy(source, target.at[core], weight_local.at[i])
        for i, (source, target) in enumerate(sources)
    ]
    for copy in local:
        copy.start()

    values = tokens[...].astype(jnp.float32)
    factor = lax.rsqrt(jnp.mean(values * values, axis=1, keepdims=True) + epsilon)
    scaled = (values * factor * gain[...]).astype(jnp.bfloat16)
    normed[...] = scaled
    for c in range(pieces):
        cut[c] = scaled[:, c * piece : (c + 1) * piece]

    gateway = at_step(half + quarter * inner)

    def block_copy(c):
        return remote(
            cut.at[c], relay_in.at[inner, c], block_send.at[c], block_recv.at[inner, c], gateway
        )

    meta_copy = remote(meta, meta_in.at[inner], meta_send.at[0], meta_recv.at[inner], gateway)

    def send_block():
        meta_copy.start()
        for c in range(pieces):
            block_copy(c).start()

    def dispatch(step):
        return remote(
            outgoing.at[step],
            received.at[step],
            out_send.at[step],
            out_recv.at[step],
            at_step(step),
        )

    def give_back(step):
        return remote(
            results.at[step],
            returned.at[step],
            back_send.at[step],
            back_recv.at[step],
            at_step(step),
        )

    pl.semaphore_wait(barrier, len(partners) + 1)

    @pl.when(inner == 1)
    def _():
        send_block()

    slots = slot_rows(meta[...], me, peers)

    def send_slots(first):
        rows = jnp.dot(
            picks(slots, range(first, first + quarter), capacity),
            normed[...],
            preferred_element_type=jnp.float32,
        ).astype(jnp.bfloat16)
        for i in range(quarter):
            block = rows[i * capacity : (i + 1) * capacity]
            if first + i == 0:
                received[0] = block
            else:
                outgoing[first + i] = block
                dispatch(first + i).start()

    send_slots(quarter)
    send_slots(0)

    @pl.when(inner == 0)
    def _():
        send_slots(half + quarter)
        send_slots(half)

    swaps = [
        remote(source, target.at[core], weight_send.at[i], weight_recv.at[i], (me, sibling))
        for i, (source, target) in enumerate(sources)
    ]
    for copy in swaps:
        copy.start()

    def relay(side, k, c):
        turn = turns[side]
        columns = pl.ds(c * piece, piece)
        return remote(
            relay_out.at[side, k, :, columns],
            received.at[k ^ turn, :, columns],
            relay_send.at[side * half + k, c],
            relay_recv.at[(k ^ turn) - half, c],
            at_step(k),
        )

    def pass_on(side):
        remote(
            meta, meta_in.at[side], meta_send.at[0], meta_recv.at[side], at_step(turns[side])
        ).wait_recv()
        picked = picks(slot_rows(meta_in[side], me, half), range(half), capacity)
        for c in range(pieces):
            columns = pl.ds(c * piece, piece)
            remote(
                cut.at[c],
                relay_in.at[side, c],
                block_send.at[c],
                block_recv.at[side, c],
                at_step(turns[side]),
            ).wait_recv()
            rows = jnp.dot(
                picked, relay_in[side, c], preferred_element_type=jnp.float32
            ).astype(jnp.bfloat16)
            received[turns[side], :, columns] = rows[:capacity]
            for k in range(half - 1, 0, -1):
                relay_out[side, k, :, columns] = rows[k * capacity : (k + 1) * capacity]
                relay(side, k, c).start()

    @pl.when(inner == 1)
    def _():
        pass_on(1)

    for i in range(len(sources)):
        local[i].wait()
        swaps[i].wait()

    def near(pair, carry):
        for i in range(2):
            step = 2 * pair + i

            @pl.when(step > 0)
            def _():
                dispatch(step).wait_recv()

        block = received[pl.ds(2 * pair, 2)].reshape(2 * capacity, width)
        out = gated_sum(block, gate_all, up_all, down_all).astype(jnp.bfloat16)
        for i in range(2):
            step = 2 * pair + i
            part = out[i * capacity : (i + 1) * capacity]

            @pl.when(step > 0)
            def _():
                results[step] = part
                give_back(step).start()

            @pl.when(step == 0)
            def _():
                returned[step] = part

        return carry

    total[...] = gated_sum(normed[...], s_gate_all, s_up_all, s_down_all)
    lax.fori_loop(0, half // 2, near, 0)

    def side_of(step):
        side = is_inner(toggled(me, step, peers))
        return side, toggled(step, half + quarter * side, peers)

    def home(step):
        side, k = side_of(step)
        return remote(
            results.at[step],
            relay_back.at[side, k],
            home_send.at[step - half],
            home_recv.at[side * half + k],
            at_step(k),
        )

    def far(pair, carry):
        start = half + (2 * pair + quarter * inner) % half
        for i in range(2):
            step = start + i
            side, k = side_of(step)

            @pl.when(side == 0)
            def _():
                dispatch(step).wait_recv()

            @pl.when((side == 1) & (k > 0))
            def _():
                for c in range(pieces):
                    columns = pl.ds(c * piece, piece)
                    remote(
                        relay_out.at[0, 1, :, columns],
                        received.at[step, :, columns],
                        relay_send.at[1, c],
                        relay_recv.at[step - half, c],
                        at_step(1),
                    ).wait_recv()

        block = received[pl.ds(start, 2)].reshape(2 * capacity, width)
        out = gated_sum(block, gate_all, up_all, down_all).astype(jnp.bfloat16)
        for i in range(2):
            step = start + i
            side, k = side_of(step)
            part = out[i * capacity : (i + 1) * capacity]

            @pl.when(side == 0)
            def _():
                results[step] = part
                give_back(step).start()

            @pl.when((side == 1) & (k > 0))
            def _():
                results[step] = part
                home(step).start()

            @pl.when((side == 1) & (k == 0))
            def _():
                relay_back[1, 0] = part

        return carry

    lax.fori_loop(0, half // 2, far, 0)

    def sums(side, c):
        return remote(
            sums_out.at[side, c],
            sums_in.at[c],
            sums_send.at[side * pieces + c],
            sums_recv.at[c],
            at_step(turns[side]),
        )

    @pl.when(inner == 1)
    def _():
        for side in (1,):
            places, scales = slot_places(meta_in[side], me, capacity)
            pair = weight_matrix(places, scales, 0, half * capacity)
            for k in range(1, half):
                remote(
                    results.at[half],
                    relay_back.at[side, k],
                    home_send.at[0],
                    home_recv.at[side * half + k],
                    at_step(k),
                ).wait_recv()
            for c in range(pieces):
                block = relay_back[side, :, :, pl.ds(c * piece, piece)]
                sums_out[side, c] = weighted(
                    pair, block.reshape(half * capacity, piece)
                ).astype(jnp.bfloat16)
                sums(side, c).start()

    places, scales = slot_places(meta[...], me, capacity)
    for step in range(1, half):
        give_back(step).wait_recv()
    pair = weight_matrix(places, scales, 0, half * capacity)
    total[...] += weighted(pair, returned[:half].reshape(half * capacity, width))

    @pl.when(inner == 1)
    def _():
        for c in range(pieces):
            sums(1, c).wait_recv()
            columns = pl.ds(c * piece, piece)
            mixed[:, columns] = (total[:, columns] + sums_in[c].astype(jnp.float32)).astype(
                jnp.bfloat16
            )

    @pl.when(inner == 0)
    def _():
        for first in (half, half + quarter):
            for i in range(quarter):
                give_back(first + i).wait_recv()
            pair = weight_matrix(places, scales, first * capacity, quarter * capacity)
            block = returned[first : first + quarter].reshape(quarter * capacity, width)
            term = total[...] + weighted(pair, block)
            if first == half:
                total[...] = term
            else:
                mixed[...] = term.astype(jnp.bfloat16)
        for step in range(half, peers):
            dispatch(step).wait_send()

    for step in range(1, half):
        dispatch(step).wait_send()
        give_back(step).wait_send()

    def settle(i, carry):
        step = half + i
        side, k = side_of(step)

        @pl.when(side == 0)
        def _():
            give_back(step).wait_send()

        @pl.when((side == 1) & (k > 0))
        def _():
            home(step).wait_send()

        return carry

    lax.fori_loop(0, half, settle, 0)

    @pl.when(inner == 1)
    def _():
        meta_copy.wait_send()
        for side in (1,):
            for c in range(pieces):
                block_copy(c).wait_send()
                sums(side, c).wait_send()
                for k in range(1, half):
                    relay(side, k, c).wait_send()


def kernel_body(
    tokens,
    norm_gain,
    expert_ids,
    route_weights,
    expert_gate,
    expert_up,
    expert_down,
    shared_gate,
    shared_up,
    shared_down,
):
    peers = lax.axis_size("ep")
    halves = lax.axis_size("tp")
    tok_rows, width = tokens.shape
    capacity = 3 * tok_rows * expert_ids.shape[1] // (2 * peers)
    half, pieces = peers // 2, 4
    vmem = pl.BlockSpec(memory_space=pltpu.VMEM)
    anywhere = pl.BlockSpec(memory_space=pl.ANY)
    weights = (
        expert_gate[0],
        expert_up[0],
        expert_down[0],
        shared_gate,
        shared_up,
        shared_down,
    )
    meta = jnp.concatenate(
        [expert_ids.astype(jnp.float32), route_weights, jnp.zeros((tok_rows, 4), jnp.float32)],
        axis=1,
    ).T

    def rows(*shape):
        return pltpu.VMEM(shape, jnp.bfloat16)

    dma = pltpu.SemaphoreType.DMA
    return pl.pallas_call(
        functools.partial(layer_kernel, peers, capacity, pieces),
        out_shape=jax.ShapeDtypeStruct((tok_rows, width), jnp.bfloat16),
        in_specs=[vmem] * 3 + [anywhere] * 6,
        out_specs=vmem,
        scratch_shapes=[pltpu.VMEM((halves,) + w.shape, w.dtype) for w in weights]
        + [
            rows(tok_rows, width),
            rows(pieces, tok_rows, width // pieces),
            rows(peers, capacity, width),
            rows(peers, capacity, width),
            rows(peers, capacity, width),
            rows(peers, capacity, width),
            pltpu.VMEM((tok_rows, width), jnp.float32),
            rows(2, pieces, tok_rows, width // pieces),
            pltpu.VMEM((2,) + meta.shape, jnp.float32),
            rows(2, half, capacity, width),
            rows(2, half, capacity, width),
            rows(2, pieces, tok_rows, width // pieces),
            rows(pieces, tok_rows, width // pieces),
        ]
        + [dma((len(weights),))] * 3
        + [dma((peers,))] * 4
        + [dma((pieces,)), dma((2, pieces)), dma((1,)), dma((2,))]
        + [dma((2 * half, pieces)), dma((half, pieces))]
        + [dma((half,)), dma((2 * half,))]
        + [dma((2 * pieces,)), dma((pieces,))],
        compiler_params=pltpu.CompilerParams(
            collective_id=0, has_side_effects=True, vmem_limit_bytes=60 * 1024 * 1024
        ),
        name="layer",
    )(tokens, norm_gain.reshape(1, width), meta, *weights)


def normalize(tokens, norm_gain):
    values = tokens.astype(jnp.float32)
    factor = lax.rsqrt(jnp.mean(values * values, axis=1, keepdims=True) + epsilon)
    return (values * factor * norm_gain[None, :]).astype(jnp.bfloat16)


def round_term(partial_value):
    return lax.optimization_barrier(partial_value.astype(jnp.bfloat16)).astype(jnp.float32)


def gated_rows(row_block, gate_w, up_w):
    gate_value = jnp.dot(row_block, gate_w, preferred_element_type=jnp.float32)
    up_value = jnp.dot(row_block, up_w, preferred_element_type=jnp.float32)
    return (jax.nn.silu(gate_value) * up_value).astype(jnp.bfloat16)


def sliced_term(hidden, down_w):
    return round_term(jnp.dot(hidden, down_w, preferred_element_type=jnp.float32))


def shared_branch(normed, shared_gate, shared_up, shared_down):
    hidden = gated_rows(lax.all_gather(normed, "tp", axis=0, tiled=True), shared_gate, shared_up)
    return lax.psum_scatter(
        sliced_term(hidden, shared_down).astype(jnp.bfloat16), "tp", scatter_dimension=0, tiled=True
    ).astype(jnp.float32)


def body(
    tokens,
    norm_gain,
    expert_ids,
    route_weights,
    expert_gate,
    expert_up,
    expert_down,
    shared_gate,
    shared_up,
    shared_down,
):
    normed = normalize(tokens, norm_gain)
    tok_rows = tokens.shape[0]
    model_width = tokens.shape[1]
    top_count = expert_ids.shape[1]
    ep_size = lax.axis_size("ep")
    experts = expert_gate.shape[0] * ep_size
    capacity = 3 * tok_rows * top_count // (2 * experts)
    assigned = tok_rows * top_count
    gate_one = expert_gate[0]
    up_one = expert_up[0]
    down_one = expert_down[0]
    flat_ids = expert_ids.reshape(-1)
    onehot = (flat_ids[:, None] == jnp.arange(experts, dtype=jnp.int32)[None, :]).astype(
        jnp.bfloat16
    )
    earlier = (jnp.arange(assigned)[:, None] > jnp.arange(assigned)[None, :]).astype(jnp.bfloat16)
    before_count = jnp.dot(earlier, onehot, preferred_element_type=jnp.float32)
    slot_index = jnp.sum(before_count * onehot.astype(jnp.float32), axis=1).astype(jnp.int32)
    position = flat_ids * capacity + slot_index
    owners = (
        jnp.full((experts * capacity,), tok_rows, jnp.int32)
        .at[position]
        .set(jnp.arange(assigned, dtype=jnp.int32) // top_count)
    )
    padded = jnp.concatenate([normed, jnp.zeros((1, model_width), jnp.bfloat16)], axis=0)
    outgoing = padded[owners].reshape(ep_size, capacity, model_width)
    half_slots = capacity // 2
    split_rows = outgoing.reshape(ep_size, 2, half_slots, model_width)
    results = []
    for portion in range(2):
        received = lax.all_to_all(
            split_rows[:, portion], "ep", split_axis=0, concat_axis=0, tiled=True
        )
        hidden = gated_rows(
            lax.all_gather(
                received.reshape(ep_size * half_slots, model_width), "tp", axis=0, tiled=True
            ),
            gate_one,
            up_one,
        )
        summed = lax.psum_scatter(
            sliced_term(hidden, down_one).astype(jnp.bfloat16),
            "tp",
            scatter_dimension=0,
            tiled=True,
        )
        results.append(
            lax.all_to_all(
                summed.reshape(ep_size, half_slots, model_width),
                "ep",
                split_axis=0,
                concat_axis=0,
                tiled=True,
            )
        )
    returned = jnp.stack(results, axis=1)
    gathered = returned.reshape(experts * capacity, model_width)[position]
    routed = jnp.sum(
        gathered.reshape(tok_rows, top_count, model_width).astype(jnp.float32)
        * route_weights[:, :, None],
        axis=1,
    )
    shared_out = shared_branch(normed, shared_gate, shared_up, shared_down)
    return (routed + shared_out).astype(jnp.bfloat16)


def plan_of(*args):
    peers = lax.axis_size("ep")
    capacity = 3 * args[0].shape[0] * args[2].shape[1] // (2 * peers)
    whole_tiles = capacity % 16 == 0 and peers % 4 == 0 and peers & (peers - 1) == 0
    fits = whole_tiles and lax.axis_size("tp") == 2 and args[4].shape[0] == 1
    return (kernel_body if fits else body)(*args)


def solution(mesh):
    placed = (
        P(("ep", "tp"), None),
        P(),
        P(("ep", "tp"), None),
        P(("ep", "tp"), None),
        P("ep", None, "tp"),
        P("ep", None, "tp"),
        P("ep", "tp", None),
        P(None, "tp"),
        P(None, "tp"),
        P("tp", None),
    )
    return jax.shard_map(
        plan_of, mesh=mesh, in_specs=placed, out_specs=P(("ep", "tp"), None), check_vma=False
    )
```

profile of v0, /device:TPU:9, one launch (start us, length us, event | category | flops | bytes accessed | tf_op | source)
XLA Modules:
  0.0 141.3 jit_solution(14975725850406835986)
XLA Ops:
  0.0 0.0 copy-start.1
  0.0 0.1 pad.2.clone
  0.1 0.6 copy-done.1
  0.7 0.0 copy-start
  0.7 0.7 copy-done
  1.4 0.7 maximum_bitcast_fusion.meta
  2.0 137.0 %layer.1 = bf16[256,2048]{1,0:T(8,128)(2,1)} custom-call(bf16[256,2048]{1,0:T(8,128)(2,1)} %tokens.1, f32[1,2048]{1,0:T(1,128)} %bitcast.9, f32[8,256]{1,0:T(8,128)} %maximum_bitcast_fusion.meta, bf16[2048,256]{1,0:T(8,128)(2,1)} %bitcast.6, bf16[2048,256]{1,0:T(8,128)(2,1)} %bitcast.7, bf16[256,2048]{1,0:T(8,128)(2,1)} %bitcast.8, ...), custom_call_target="tpu_custom_call" | custom-call | tf_op jit(solution)/shard_map/layer/pallas_call | solution.py:524
  139.0 2.3 %copy.12 = bf16[256,2048]{1,0:T(8,128)(2,1)} copy(bf16[256,2048]{1,0:T(8,128)(2,1)} %layer.1) | data formatting | bytes 2097152
  (2 shorter events, 0.0 us)
Async XLA Ops:
  0.0 0.7 copy-start.1
  0.7 0.7 copy-start
where the time goes:
time: 143 us; the launch traced here: 141 us
  Pallas kernels  137 us (96%)
  local copies, waits for them, and re-layouts  3.66 us (3%)
    pallas_call x1, Pallas kernels, kernel_body(): pl.pallas_call(functools.partial(layer_kernel, peers, capacity, pieces),...  137 us
    unnamed x5, local copies, waits for them, and re-layouts  3.58 us

commit v1 on v0

--- a/solution.py
+++ b/solution.py
@@ -90,6 +90,9 @@
     return jnp.dot(pair[0], block, preferred_element_type=jnp.float32) + jnp.dot(
         pair[1], block, preferred_element_type=jnp.float32
     )
+
+
+ORDER = "1S2A3B4F5XGabYN"
 
 
 def layer_kernel(
@@ -113,14 +116,16 @@
     s_up_all,
     s_down_all,
     normed,
-    cut,
     outgoing,
-    received,
-    results,
+    near_in,
+    far_in,
+    near_out,
+    far_out,
     returned,
     total,
     relay_in,
     meta_in,
+    picked,
     relay_out,
     relay_back,
     sums_out,
@@ -149,15 +154,14 @@
     width = tokens.shape[1]
     piece = width // pieces
     half, quarter = peers // 2, peers // 4
-
-    def is_inner(index):
-        return ((index // quarter + 1) // 2) % 2
-
-    inner = is_inner(me)
+    inner = ((me // quarter + 1) // 2) % 2
     turns = (half, half + quarter)
 
     def at_step(step):
         return (toggled(me, step, peers), core)
+
+    def columns(c):
+        return pl.ds(c * piece, piece)
 
     def remote(source, target, send, recv, place):
         return pltpu.make_async_remote_copy(
@@ -170,9 +174,9 @@
         )
 
     barrier = pltpu.get_barrier_semaphore()
-    partners = range(1, peers)
+    greeted = range(1, peers)
     pl.semaphore_signal(barrier, inc=1, device_id=(me, sibling), device_id_type=MESH)
-    for step in partners:
+    for step in greeted:
         pl.semaphore_signal(barrier, inc=1, device_id=at_step(step), device_id_type=MESH)
     sources = (
         (shared_gate, s_gate_all),
@@ -186,55 +190,83 @@
         pltpu.make_async_copy(source, target.at[core], weight_local.at[i])
         for i, (source, target) in enumerate(sources)
     ]
+    swaps = [
+        remote(source, target.at[core], weight_send.at[i], weight_recv.at[i], (me, sibling))
+        for i, (source, target) in enumerate(sources)
+    ]
     for copy in local:
         copy.start()
 
     values = tokens[...].astype(jnp.float32)
     factor = lax.rsqrt(jnp.mean(values * values, axis=1, keepdims=True) + epsilon)
-    scaled = (values * factor * gain[...]).astype(jnp.bfloat16)
-    normed[...] = scaled
-    for c in range(pieces):
-        cut[c] = scaled[:, c * piece : (c + 1) * piece]
+    normed[...] = (values * factor * gain[...]).astype(jnp.bfloat16)
 
     gateway = at_step(half + quarter * inner)
+    meta_copy = remote(meta, meta_in.at[inner], meta_send.at[0], meta_recv.at[inner], gateway)
 
     def block_copy(c):
         return remote(
-            cut.at[c], relay_in.at[inner, c], block_send.at[c], block_recv.at[inner, c], gateway
-        )
-
-    meta_copy = remote(meta, meta_in.at[inner], meta_send.at[0], meta_recv.at[inner], gateway)
+            normed.at[:, columns(c)],
+            relay_in.at[inner, :, columns(c)],
+            block_send.at[c],
+            block_recv.at[inner, c],
+            gateway,
+        )
 
     def send_block():
-        meta_copy.start()
         for c in range(pieces):
             block_copy(c).start()
 
     def dispatch(step):
         return remote(
-            outgoing.at[step],
-            received.at[step],
-            out_send.at[step],
-            out_recv.at[step],
-            at_step(step),
+            outgoing.at[step], near_in.at[step], out_send.at[step], out_recv.at[step], at_step(step)
         )
 
     def give_back(step):
         return remote(
-            results.at[step],
+            near_out.at[step],
             returned.at[step],
             back_send.at[step],
             back_recv.at[step],
             at_step(step),
         )
 
-    pl.semaphore_wait(barrier, len(partners) + 1)
-
-    @pl.when(inner == 1)
-    def _():
-        send_block()
-
-    slots = slot_rows(meta[...], me, peers)
+    def relay(side, k, c):
+        return remote(
+            relay_out.at[side, k, :, columns(c)],
+            far_in.at[side, k % quarter, :, columns(c)],
+            relay_send.at[side * half + k, c],
+            relay_recv.at[side * quarter + k % quarter, c],
+            at_step(k),
+        )
+
+    def home(side, j):
+        k = j + quarter * (1 - inner)
+        return remote(
+            far_out.at[side, j],
+            relay_back.at[side, k],
+            home_send.at[side * quarter + j],
+            home_recv.at[side * half + k],
+            at_step(k),
+        )
+
+    def sums(side, c):
+        return remote(
+            sums_out.at[side, :, columns(c)],
+            sums_in.at[:, columns(c)],
+            sums_send.at[side * pieces + c],
+            sums_recv.at[c],
+            at_step(turns[side]),
+        )
+
+    def on_inner(action):
+        pl.when(inner == 1)(action)
+
+    pl.semaphore_wait(barrier, len(greeted) + 1)
+    meta_copy.start()
+    on_inner(send_block)
+
+    slots = slot_rows(meta[...], me, half)
 
     def send_slots(first):
         rows = jnp.dot(
@@ -245,241 +277,176 @@
         for i in range(quarter):
             block = rows[i * capacity : (i + 1) * capacity]
             if first + i == 0:
-                received[0] = block
+                near_in[0] = block
             else:
                 outgoing[first + i] = block
                 dispatch(first + i).start()
 
     send_slots(quarter)
     send_slots(0)
-
-    @pl.when(inner == 0)
-    def _():
-        send_slots(half + quarter)
-        send_slots(half)
-
-    swaps = [
-        remote(source, target.at[core], weight_send.at[i], weight_recv.at[i], (me, sibling))
-        for i, (source, target) in enumerate(sources)
-    ]
+    pl.when(inner == 0)(send_block)
     for copy in swaps:
         copy.start()
 
-    def relay(side, k, c):
-        turn = turns[side]
-        columns = pl.ds(c * piece, piece)
-        return remote(
-            relay_out.at[side, k, :, columns],
-            received.at[k ^ turn, :, columns],
-            relay_send.at[side * half + k, c],
-            relay_recv.at[(k ^ turn) - half, c],
-            at_step(k),
-        )
-
-    def pass_on(side):
+    def open_side(side):
         remote(
             meta, meta_in.at[side], meta_send.at[0], meta_recv.at[side], at_step(turns[side])
         ).wait_recv()
-        picked = picks(slot_rows(meta_in[side], me, half), range(half), capacity)
+        picked[side] = picks(slot_rows(meta_in[side], me, half), range(half), capacity)
+
+    def pass_on(side, c):
+        remote(
+            normed.at[:, columns(c)],
+            relay_in.at[side, :, columns(c)],
+            block_send.at[c],
+            block_recv.at[side, c],
+            at_step(turns[side]),
+        ).wait_recv()
+        rows = jnp.dot(
+            picked[side], relay_in[side, :, columns(c)], preferred_element_type=jnp.float32
+        ).astype(jnp.bfloat16)
+        far_in[side, 0, :, columns(c)] = rows[:capacity]
+        for k in range(half - 1, 0, -1):
+            relay_out[side, k, :, columns(c)] = rows[k * capacity : (k + 1) * capacity]
+            relay(side, k, c).start()
+
+    def pass_some(side, chunks):
+        def action():
+            if chunks[0] == 0:
+                open_side(side)
+            for c in chunks:
+                pass_on(side, c)
+
+        on_inner(action)
+
+    def near(group):
+        steps = range(group * quarter, (group + 1) * quarter)
+        for step in steps:
+            if step > 0:
+                dispatch(step).wait_recv()
+        block = near_in[group * quarter : (group + 1) * quarter].reshape(quarter * capacity, width)
+        out = gated_sum(block, gate_all, up_all, down_all).astype(jnp.bfloat16)
+        for i, step in enumerate(steps):
+            part = out[i * capacity : (i + 1) * capacity]
+            if step == 0:
+                returned[0] = part
+            else:
+                near_out[step] = part
+
+    def near_send(group):
+        for step in range(group * quarter, (group + 1) * quarter):
+            if step > 0:
+                give_back(step).start()
+
+    def far_wait(side, j):
         for c in range(pieces):
-            columns = pl.ds(c * piece, piece)
             remote(
-                cut.at[c],
-                relay_in.at[side, c],
-                block_send.at[c],
-                block_recv.at[side, c],
-                at_step(turns[side]),
+                relay_out.at[side, 1, :, columns(c)],
+                far_in.at[side, j, :, columns(c)],
+                relay_send.at[side * half + 1, c],
+                relay_recv.at[side * quarter + j, c],
+                at_step(1),
             ).wait_recv()
-            rows = jnp.dot(
-                picked, relay_in[side, c], preferred_element_type=jnp.float32
+
+    def far(side):
+        pl.when(inner == 0)(lambda: far_wait(side, 0))
+        for j in range(1, quarter):
+            far_wait(side, j)
+        block = far_in[side].reshape(quarter * capacity, width)
+        out = gated_sum(block, gate_all, up_all, down_all).astype(jnp.bfloat16)
+        for j in range(quarter - 1, -1, -1):
+            part = out[j * capacity : (j + 1) * capacity]
+            far_out[side, j] = part
+            if j == 0:
+
+                @pl.when(inner == 0)
+                def _():
+                    home(side, 0).start()
+
+                @pl.when(inner == 1)
+                def _():
+                    relay_back[side, 0] = far_out[side, 0]
+            else:
+                home(side, j).start()
+
+    def send_sums(side):
+        places, scales = slot_places(meta_in[side], me, capacity)
+        pair = weight_matrix(places, scales, 0, half * capacity)
+        for k in range(1, half):
+            remote(
+                far_out.at[side, 1],
+                relay_back.at[side, k],
+                home_send.at[side * quarter + 1],
+                home_recv.at[side * half + k],
+                at_step(k),
+            ).wait_recv()
+        for c in range(pieces):
+            block = relay_back[side, :, :, columns(c)]
+            sums_out[side, :, columns(c)] = weighted(
+                pair, block.reshape(half * capacity, piece)
             ).astype(jnp.bfloat16)
-            received[turns[side], :, columns] = rows[:capacity]
-            for k in range(half - 1, 0, -1):
-                relay_out[side, k, :, columns] = rows[k * capacity : (k + 1) * capacity]
-                relay(side, k, c).start()
-
-    @pl.when(inner == 1)
-    def _():
-        pass_on(1)
-
-    for i in range(len(sources)):
-        local[i].wait()
-        swaps[i].wait()
-
-    def near(pair, carry):
-        for i in range(2):
-            step = 2 * pair + i
-
-            @pl.when(step > 0)
-            def _():
-                dispatch(step).wait_recv()
-
-        block = received[pl.ds(2 * pair, 2)].reshape(2 * capacity, width)
-        out = gated_sum(block, gate_all, up_all, down_all).astype(jnp.bfloat16)
-        for i in range(2):
-            step = 2 * pair + i
-            part = out[i * capacity : (i + 1) * capacity]
-
-            @pl.when(step > 0)
-            def _():
-                results[step] = part
-                give_back(step).start()
-
-            @pl.when(step == 0)
-            def _():
-                returned[step] = part
-
-        return carry
-
-    total[...] = gated_sum(normed[...], s_gate_all, s_up_all, s_down_all)
-    lax.fori_loop(0, half // 2, near, 0)
-
-    def side_of(step):
-        side = is_inner(toggled(me, step, peers))
-        return side, toggled(step, half + quarter * side, peers)
-
-    def home(step):
-        side, k = side_of(step)
-        return remote(
-            results.at[step],
-            relay_back.at[side, k],
-            home_send.at[step - half],
-            home_recv.at[side * half + k],
-            at_step(k),
-        )
-
-    def far(pair, carry):
-        start = half + (2 * pair + quarter * inner) % half
-        for i in range(2):
-            step = start + i
-            side, k = side_of(step)
-
-            @pl.when(side == 0)
-            def _():
-                dispatch(step).wait_recv()
-
-            @pl.when((side == 1) & (k > 0))
-            def _():
-                for c in range(pieces):
-                    columns = pl.ds(c * piece, piece)
-                    remote(
-                        relay_out.at[0, 1, :, columns],
-                        received.at[step, :, columns],
-                        relay_send.at[1, c],
-                        relay_recv.at[step - half, c],
-                        at_step(1),
-                    ).wait_recv()
-
-        block = received[pl.ds(start, 2)].reshape(2 * capacity, width)
-        out = gated_sum(block, gate_all, up_all, down_all).astype(jnp.bfloat16)
-        for i in range(2):
-            step = start + i
-            side, k = side_of(step)
-            part = out[i * capacity : (i + 1) * capacity]
-
-            @pl.when(side == 0)
-            def _():
-                results[step] = part
-                give_back(step).start()
-
-            @pl.when((side == 1) & (k > 0))
-            def _():
-                results[step] = part
-                home(step).start()
-
-            @pl.when((side == 1) & (k == 0))
-            def _():
-                relay_back[1, 0] = part
-
-        return carry
-
-    lax.fori_loop(0, half // 2, far, 0)
-
-    def sums(side, c):
-        return remote(
-            sums_out.at[side, c],
-            sums_in.at[c],
-            sums_send.at[side * pieces + c],
+            sums(side, c).start()
+
+    def shared():
+        for i in range(len(sources)):
+            local[i].wait()
+            swaps[i].wait()
+        total[...] = gated_sum(normed[...], s_gate_all, s_up_all, s_down_all)
+
+    def near_total():
+        places, scales = slot_places(meta[...], me, capacity)
+        pair = weight_matrix(places, scales, 0, half * capacity)
+        for step in range(1, half):
+            give_back(step).wait_recv()
+        total[...] += weighted(pair, returned[...].reshape(half * capacity, width))
+
+    actions = {
+        "S": shared,
+        "A": lambda: near(0),
+        "B": lambda: near(1),
+        "a": lambda: near_send(0),
+        "b": lambda: near_send(1),
+        "F": lambda: far(1),
+        "G": lambda: far(0),
+        "1": lambda: pass_some(1, (0, 1)),
+        "2": lambda: pass_some(1, (2,)),
+        "3": lambda: pass_some(1, (3,)),
+        "4": lambda: pass_some(0, (0, 1)),
+        "5": lambda: pass_some(0, (2, 3)),
+        "X": lambda: on_inner(lambda: send_sums(1)),
+        "Y": lambda: on_inner(lambda: send_sums(0)),
+        "N": near_total,
+    }
+    for name in ORDER:
+        actions[name]()
+
+    for c in range(pieces):
+        remote(
+            sums_out.at[0, :, columns(c)],
+            sums_in.at[:, columns(c)],
+            sums_send.at[c],
             sums_recv.at[c],
-            at_step(turns[side]),
-        )
-
-    @pl.when(inner == 1)
-    def _():
-        for side in (1,):
-            places, scales = slot_places(meta_in[side], me, capacity)
-            pair = weight_matrix(places, scales, 0, half * capacity)
-            for k in range(1, half):
-                remote(
-                    results.at[half],
-                    relay_back.at[side, k],
-                    home_send.at[0],
-                    home_recv.at[side * half + k],
-                    at_step(k),
-                ).wait_recv()
-            for c in range(pieces):
-                block = relay_back[side, :, :, pl.ds(c * piece, piece)]
-                sums_out[side, c] = weighted(
-                    pair, block.reshape(half * capacity, piece)
-                ).astype(jnp.bfloat16)
-                sums(side, c).start()
-
-    places, scales = slot_places(meta[...], me, capacity)
-    for step in range(1, half):
-        give_back(step).wait_recv()
-    pair = weight_matrix(places, scales, 0, half * capacity)
-    total[...] += weighted(pair, returned[:half].reshape(half * capacity, width))
-
-    @pl.when(inner == 1)
-    def _():
-        for c in range(pieces):
-            sums(1, c).wait_recv()
-            columns = pl.ds(c * piece, piece)
-            mixed[:, columns] = (total[:, columns] + sums_in[c].astype(jnp.float32)).astype(
-                jnp.bfloat16
-            )
-
-    @pl.when(inner == 0)
-    def _():
-        for first in (half, half + quarter):
-            for i in range(quarter):
-                give_back(first + i).wait_recv()
-            pair = weight_matrix(places, scales, first * capacity, quarter * capacity)
-            block = returned[first : first + quarter].reshape(quarter * capacity, width)
-            term = total[...] + weighted(pair, block)
-            if first == half:
-                total[...] = term
-            else:
-                mixed[...] = term.astype(jnp.bfloat16)
-        for step in range(half, peers):
-            dispatch(step).wait_send()
-
+            gateway,
+        ).wait_recv()
+        mixed[:, columns(c)] = (
+            total[:, columns(c)] + sums_in[:, columns(c)].astype(jnp.float32)
+        ).astype(jnp.bfloat16)
+
+    meta_copy.wait_send()
+    for c in range(pieces):
+        block_copy(c).wait_send()
     for step in range(1, half):
         dispatch(step).wait_send()
         give_back(step).wait_send()
-
-    def settle(i, carry):
-        step = half + i
-        side, k = side_of(step)
-
-        @pl.when(side == 0)
-        def _():
-            give_back(step).wait_send()
-
-        @pl.when((side == 1) & (k > 0))
-        def _():
-            home(step).wait_send()
-
-        return carry
-
-    lax.fori_loop(0, half, settle, 0)
+    for side in range(2):
+        pl.when(inner == 0)(lambda: home(side, 0).wait_send())
+        for j in range(1, quarter):
+            home(side, j).wait_send()
 
     @pl.when(inner == 1)
     def _():
-        meta_copy.wait_send()
-        for side in (1,):
+        for side in range(2):
             for c in range(pieces):
-                block_copy(c).wait_send()
                 sums(side, c).wait_send()
                 for k in range(1, half):
                     relay(side, k, c).wait_send()
@@ -501,7 +468,7 @@
     halves = lax.axis_size("tp")
     tok_rows, width = tokens.shape
     capacity = 3 * tok_rows * expert_ids.shape[1] // (2 * peers)
-    half, pieces = peers // 2, 4
+    half, quarter, pieces = peers // 2, peers // 4, 4
     vmem = pl.BlockSpec(memory_space=pltpu.VMEM)
     anywhere = pl.BlockSpec(memory_space=pl.ANY)
     weights = (
@@ -529,24 +496,26 @@
         scratch_shapes=[pltpu.VMEM((halves,) + w.shape, w.dtype) for w in weights]
         + [
             rows(tok_rows, width),
-            rows(pieces, tok_rows, width // pieces),
-            rows(peers, capacity, width),
-            rows(peers, capacity, width),
-            rows(peers, capacity, width),
-            rows(peers, capacity, width),
+            rows(half, capacity, width),
+            rows(half, capacity, width),
+            rows(2, quarter, capacity, width),
+            rows(half, capacity, width),
+            rows(2, quarter, capacity, width),
+            rows(half, capacity, width),
             pltpu.VMEM((tok_rows, width), jnp.float32),
-            rows(2, pieces, tok_rows, width // pieces),
+            rows(2, tok_rows, width),
             pltpu.VMEM((2,) + meta.shape, jnp.float32),
+            rows(2, half * capacity, tok_rows),
             rows(2, half, capacity, width),
             rows(2, half, capacity, width),
-            rows(2, pieces, tok_rows, width // pieces),
-            rows(pieces, tok_rows, width // pieces),
+            rows(2, tok_rows, width),
+            rows(tok_rows, width),
         ]
         + [dma((len(weights),))] * 3
-        + [dma((peers,))] * 4
+        + [dma((half,))] * 4
         + [dma((pieces,)), dma((2, pieces)), dma((1,)), dma((2,))]
-        + [dma((2 * half, pieces)), dma((half, pieces))]
-        + [dma((half,)), dma((2 * half,))]
+        + [dma((2 * half, pieces)), dma((2 * quarter, pieces))]
+        + [dma((2 * quarter,)), dma((2 * half,))]
         + [dma((2 * pieces,)), dma((pieces,))],
         compiler_params=pltpu.CompilerParams(
             collective_id=0, has_side_effects=True, vmem_limit_bytes=60 * 1024 * 1024

time: 143 us -> 144 us (level)
  the two profiles are of different devices: /device:TPU:9 before, /device:TPU:0 now
where the time goes in v1:
time: 144 us
  Pallas kernels  140 us (97%)
  local copies, waits for them, and re-layouts  3.66 us (3%)
    pallas_call x1, Pallas kernels, kernel_body(): pl.pallas_call(functools.partial(layer_kernel, peers, capacity, pieces),...  140 us
    unnamed x5, local copies, waits for them, and re-layouts  3.58 us

profile of v1, /device:TPU:0, one launch (start us, length us, event | category | flops | bytes accessed | tf_op | source)
XLA Modules:
  0.0 143.9 jit_solution(6011906087217193546)
XLA Ops:
  0.0 0.0 copy-start.1
  0.0 0.1 pad.2.clone
  0.1 0.6 copy-done.1
  0.7 0.0 copy-start
  0.7 0.7 copy-done
  1.4 0.7 maximum_bitcast_fusion.meta
  2.0 139.5 %layer.1 = bf16[256,2048]{1,0:T(8,128)(2,1)} custom-call(bf16[256,2048]{1,0:T(8,128)(2,1)} %tokens.1, f32[1,2048]{1,0:T(1,128)} %bitcast.9, f32[8,256]{1,0:T(8,128)} %maximum_bitcast_fusion.meta, bf16[2048,256]{1,0:T(8,128)(2,1)} %bitcast.6, bf16[2048,256]{1,0:T(8,128)(2,1)} %bitcast.7, bf16[256,2048]{1,0:T(8,128)(2,1)} %bitcast.8, ...), custom_call_target="tpu_custom_call" | custom-call | tf_op jit(solution)/shard_map/layer/pallas_call | solution.py:491
  141.6 2.3 %copy.12 = bf16[256,2048]{1,0:T(8,128)(2,1)} copy(bf16[256,2048]{1,0:T(8,128)(2,1)} %layer.1) | data formatting | bytes 2097152
  (2 shorter events, 0.0 us)
Async XLA Ops:
  0.0 0.7 copy-start.1
  0.7 0.7 copy-start

commit v2 on v1

--- a/solution.py
+++ b/solution.py
@@ -92,30 +92,45 @@
     )
 
 
-ORDER = "1S2A3B4F5XGabYN"
+PIECES = 8
+VMEM_MIB = 60
+CUTS = 8
+OWN_FIRST = 2
+ORDER = (
+    "2.0", "2.1", "2.2", "2.3", "0.0", "0.1", "S", "2.4", "2.5", "0.2", "0.3", "2.6", "2.7", "A",
+    "0.4", "0.5", "B", "0.6", "0.7", "1.0", "1.1", "F.0", "W.0", "P.0", "1.2", "1.3", "P.2", "1.4",
+    "1.5", "m", "Y.0", "Y.1", "1.6", "1.7", "Y.2", "Y.3", "F.1", "W.1", "a", "h", "W.2", "Y.4",
+    "Y.5", "Y.6", "Y.7", "P.1", "V.0", "V.1", "V.2", "V.3", "V.4", "V.5", "X.0", "X.1", "X.2",
+    "X.3", "V.6", "V.7", "X.4", "X.5", "X.6", "X.7", "N", "M",
+)
 
 
 def layer_kernel(
     peers,
     capacity,
     pieces,
+    cuts,
     tokens,
     gain,
-    meta,
+    expert_ids,
+    route_weights,
     expert_gate,
     expert_up,
     expert_down,
     shared_gate,
     shared_up,
     shared_down,
-    mixed,
+    held,
+    sums_in,
     gate_all,
     up_all,
     down_all,
     s_gate_all,
     s_up_all,
     s_down_all,
+    raw,
     normed,
+    meta,
     outgoing,
     near_in,
     far_in,
@@ -126,10 +141,14 @@
     relay_in,
     meta_in,
     picked,
+    scales_of,
     relay_out,
     relay_back,
     sums_out,
-    sums_in,
+    pass_in,
+    pass_out,
+    around,
+    token_sems,
     weight_local,
     weight_send,
     weight_recv,
@@ -147,21 +166,45 @@
     home_recv,
     sums_send,
     sums_recv,
+    pass_send,
+    pass_recv,
+    middle_send,
+    middle_recv,
+    side_send,
+    side_recv,
+    up_send,
+    held_send,
 ):
     me = lax.axis_index("ep")
     core = lax.axis_index("tp")
     sibling = 1 - core
-    width = tokens.shape[1]
-    piece = width // pieces
+    tok_rows, width = normed.shape
+    piece, cut = width // pieces, width // cuts
     half, quarter = peers // 2, peers // 4
     inner = ((me // quarter + 1) // 2) % 2
-    turns = (half, half + quarter)
+    far_turn, next_turn = half + quarter, quarter
+    turns = (half, half + quarter, quarter)
 
     def at_step(step):
         return (toggled(me, step, peers), core)
 
     def columns(c):
         return pl.ds(c * piece, piece)
+
+    def cut_columns(c):
+        return pl.ds(c * cut, cut)
+
+    def left(source, sem):
+        remote(source, source, sem, sem, at_step(1)).wait_send()
+
+    def landed(target, sem):
+        remote(target, target, sem, sem, at_step(1)).wait_recv()
+
+    def on_inner(action):
+        pl.when(inner == 1)(action)
+
+    def on_outer(action):
+        pl.when(inner == 0)(action)
 
     def remote(source, target, send, recv, place):
         return pltpu.make_async_remote_copy(
@@ -174,10 +217,20 @@
         )
 
     barrier = pltpu.get_barrier_semaphore()
-    greeted = range(1, peers)
+    greeted = [step for step in range(1, half)] + [half, far_turn]
     pl.semaphore_signal(barrier, inc=1, device_id=(me, sibling), device_id_type=MESH)
     for step in greeted:
         pl.semaphore_signal(barrier, inc=1, device_id=at_step(step), device_id_type=MESH)
+    bands = token_sems.shape[0]
+    band = tok_rows // bands
+    fetched = [
+        pltpu.make_async_copy(
+            tokens.at[pl.ds(i * band, band)], raw.at[pl.ds(i * band, band)], token_sems.at[i]
+        )
+        for i in range(bands)
+    ]
+    for copy in fetched:
+        copy.start()
     sources = (
         (shared_gate, s_gate_all),
         (shared_up, s_up_all),
@@ -194,78 +247,163 @@
         remote(source, target.at[core], weight_send.at[i], weight_recv.at[i], (me, sibling))
         for i, (source, target) in enumerate(sources)
     ]
+
+    def normalize_rows():
+        for i in range(bands):
+            fetched[i].wait()
+            at = pl.ds(i * band, band)
+            values = raw[at].astype(jnp.float32)
+            factor = lax.rsqrt(jnp.mean(values * values, axis=1, keepdims=True) + epsilon)
+            normed[at] = (values * factor * gain[...]).astype(jnp.bfloat16)
+
+    with jax.named_scope("norm"):
+        normalize_rows()
+    meta[0:2] = expert_ids[...].astype(jnp.float32)
+    meta[2:4] = route_weights[...]
+    meta[4:8] = jnp.zeros((4, tok_rows), jnp.float32)
+
+    def meta_copy(side):
+        step = {0: half, 1: far_turn, 2: next_turn}[side]
+        number = 1 if side == 0 else 0
+        return remote(
+            meta, meta_in.at[side], meta_send.at[number], meta_recv.at[side], at_step(step)
+        )
+
+    def block_copy(side, c):
+        return remote(
+            normed.at[:, columns(c)],
+            relay_in.at[side, :, columns(c)],
+            block_send.at[0],
+            block_recv.at[side, c],
+            at_step(far_turn if side == 1 else next_turn),
+        )
+
+    def forward(c):
+        return remote(
+            relay_in.at[2, :, columns(c)],
+            relay_in.at[0, :, columns(c)],
+            block_send.at[1],
+            block_recv.at[0, c],
+            at_step(far_turn),
+        )
+
+    def dispatch(step):
+        group = step // quarter
+        return remote(
+            outgoing.at[step],
+            near_in.at[step],
+            out_send.at[group],
+            out_recv.at[group],
+            at_step(step),
+        )
+
+    def give_back(step):
+        return remote(
+            near_out.at[step],
+            returned.at[step],
+            back_send.at[0],
+            back_recv.at[0],
+            at_step(step),
+        )
+
+    def relay(side, k, c):
+        target = near_in.at[k + quarter] if side == 2 else far_in.at[side, k % quarter]
+        return remote(
+            relay_out.at[side, k, :, columns(c)],
+            target.at[:, columns(c)],
+            relay_send.at[side],
+            relay_recv.at[side],
+            at_step(k),
+        )
+
+    def home(side, j, c):
+        k = j + quarter * (1 - inner)
+        return remote(
+            far_out.at[side, j, :, cut_columns(c)],
+            relay_back.at[side, k, :, cut_columns(c)],
+            home_send.at[side],
+            home_recv.at[side, c],
+            at_step(k),
+        )
+
+    def sideways(side, j, c):
+        source = near_out.at[quarter + j] if side == 2 else far_out.at[side, j]
+        return remote(
+            source.at[:, cut_columns(c)],
+            around.at[side, j, :, cut_columns(c)],
+            side_send.at[side],
+            side_recv.at[side, c],
+            at_step(j),
+        )
+
+    def upward(side, j, c):
+        if side == 2:
+            target, recv = returned.at[quarter + j], back_recv.at[1]
+        else:
+            target, recv = relay_back.at[side, quarter + j], home_recv.at[side, c]
+        return remote(
+            around.at[side, j, :, cut_columns(c)],
+            target.at[:, cut_columns(c)],
+            up_send.at[side],
+            recv,
+            at_step(next_turn),
+        )
+
+    def straight(c):
+        return remote(
+            near_out.at[quarter, :, cut_columns(c)],
+            returned.at[quarter, :, cut_columns(c)],
+            up_send.at[3],
+            back_recv.at[1],
+            at_step(next_turn),
+        )
+
+    def middle(j):
+        return remote(
+            near_out.at[quarter + j],
+            relay_back.at[2, j],
+            middle_send.at[0],
+            middle_recv.at[0],
+            at_step(j),
+        )
+
+    def sums(side, c):
+        target = pass_in if side == 0 else sums_in
+        return remote(
+            sums_out.at[side, :, cut_columns(c)],
+            target.at[:, cut_columns(c)],
+            sums_send.at[side],
+            pass_recv.at[c] if side == 0 else sums_recv.at[c],
+            at_step(far_turn),
+        )
+
+    def sums_on(c):
+        return remote(
+            pass_out.at[:, cut_columns(c)],
+            sums_in.at[:, cut_columns(c)],
+            pass_send.at[0],
+            sums_recv.at[c],
+            at_step(next_turn),
+        )
+
+    with jax.named_scope("meet"):
+        pl.semaphore_wait(barrier, len(greeted) + 1)
+
+    @pl.when(inner == 1)
+    def _():
+        meta_copy(1).start()
+        for c in range(OWN_FIRST):
+            block_copy(1, c).start()
+
+    @pl.when(inner == 0)
+    def _():
+        meta_copy(2).start()
+        meta_copy(0).start()
+        for c in range(pieces):
+            block_copy(2, c).start()
+
     for copy in local:
         copy.start()
-
-    values = tokens[...].astype(jnp.float32)
-    factor = lax.rsqrt(jnp.mean(values * values, axis=1, keepdims=True) + epsilon)
-    normed[...] = (values * factor * gain[...]).astype(jnp.bfloat16)
-
-    gateway = at_step(half + quarter * inner)
-    meta_copy = remote(meta, meta_in.at[inner], meta_send.at[0], meta_recv.at[inner], gateway)
-
-    def block_copy(c):
-        return remote(
-            normed.at[:, columns(c)],
-            relay_in.at[inner, :, columns(c)],
-            block_send.at[c],
-            block_recv.at[inner, c],
-            gateway,
-        )
-
-    def send_block():
-        for c in range(pieces):
-            block_copy(c).start()
-
-    def dispatch(step):
-        return remote(
-            outgoing.at[step], near_in.at[step], out_send.at[step], out_recv.at[step], at_step(step)
-        )
-
-    def give_back(step):
-        return remote(
-            near_out.at[step],
-            returned.at[step],
-            back_send.at[step],
-            back_recv.at[step],
-            at_step(step),
-        )
-
-    def relay(side, k, c):
-        return remote(
-            relay_out.at[side, k, :, columns(c)],
-            far_in.at[side, k % quarter, :, columns(c)],
-            relay_send.at[side * half + k, c],
-            relay_recv.at[side * quarter + k % quarter, c],
-            at_step(k),
-        )
-
-    def home(side, j):
-        k = j + quarter * (1 - inner)
-        return remote(
-            far_out.at[side, j],
-            relay_back.at[side, k],
-            home_send.at[side * quarter + j],
-            home_recv.at[side * half + k],
-            at_step(k),
-        )
-
-    def sums(side, c):
-        return remote(
-            sums_out.at[side, :, columns(c)],
-            sums_in.at[:, columns(c)],
-            sums_send.at[side * pieces + c],
-            sums_recv.at[c],
-            at_step(turns[side]),
-        )
-
-    def on_inner(action):
-        pl.when(inner == 1)(action)
-
-    pl.semaphore_wait(barrier, len(greeted) + 1)
-    meta_copy.start()
-    on_inner(send_block)
-
     slots = slot_rows(meta[...], me, half)
 
     def send_slots(first):
@@ -282,48 +420,51 @@
                 outgoing[first + i] = block
                 dispatch(first + i).start()
 
-    send_slots(quarter)
+    on_inner(lambda: send_slots(quarter))
     send_slots(0)
-    pl.when(inner == 0)(send_block)
     for copy in swaps:
         copy.start()
 
     def open_side(side):
-        remote(
-            meta, meta_in.at[side], meta_send.at[0], meta_recv.at[side], at_step(turns[side])
-        ).wait_recv()
-        picked[side] = picks(slot_rows(meta_in[side], me, half), range(half), capacity)
+        landed(meta_in.at[side], meta_recv.at[side])
+        reach = quarter if side == 2 else half
+        picked[side, : reach * capacity] = picks(
+            slot_rows(meta_in[side], me, half), range(reach), capacity
+        )
 
     def pass_on(side, c):
-        remote(
-            normed.at[:, columns(c)],
-            relay_in.at[side, :, columns(c)],
-            block_send.at[c],
-            block_recv.at[side, c],
-            at_step(turns[side]),
-        ).wait_recv()
+        if c == 0:
+            open_side(side)
+        reach = quarter if side == 2 else half
+        landed(relay_in.at[side, :, columns(c)], block_recv.at[side, c])
+        if side == 2:
+            forward(c).start()
+            if c == pieces - 1:
+                for own in range(OWN_FIRST, pieces):
+                    block_copy(1, own).start()
         rows = jnp.dot(
-            picked[side], relay_in[side, :, columns(c)], preferred_element_type=jnp.float32
+            picked[side, : reach * capacity],
+            relay_in[side, :, columns(c)],
+            preferred_element_type=jnp.float32,
         ).astype(jnp.bfloat16)
-        far_in[side, 0, :, columns(c)] = rows[:capacity]
-        for k in range(half - 1, 0, -1):
+        if side == 2:
+            near_in[quarter, :, columns(c)] = rows[:capacity]
+        else:
+            far_in[side, 0, :, columns(c)] = rows[:capacity]
+        for k in range(reach - 1, 0, -1):
             relay_out[side, k, :, columns(c)] = rows[k * capacity : (k + 1) * capacity]
             relay(side, k, c).start()
 
-    def pass_some(side, chunks):
-        def action():
-            if chunks[0] == 0:
-                open_side(side)
-            for c in chunks:
-                pass_on(side, c)
-
-        on_inner(action)
-
     def near(group):
         steps = range(group * quarter, (group + 1) * quarter)
-        for step in steps:
-            if step > 0:
-                dispatch(step).wait_recv()
+        if group == 0:
+            landed(near_in.at[pl.ds(1, quarter - 1)], out_recv.at[0])
+        else:
+            on_outer(lambda: landed(near_in.at[pl.ds(quarter, quarter)], out_recv.at[1]))
+            on_inner(
+                lambda: landed(near_in.at[pl.ds(quarter + 1, quarter - 1)], relay_recv.at[2])
+            )
+
         block = near_in[group * quarter : (group + 1) * quarter].reshape(quarter * capacity, width)
         out = gated_sum(block, gate_all, up_all, down_all).astype(jnp.bfloat16)
         for i, step in enumerate(steps):
@@ -333,59 +474,76 @@
             else:
                 near_out[step] = part
 
-    def near_send(group):
-        for step in range(group * quarter, (group + 1) * quarter):
-            if step > 0:
-                give_back(step).start()
-
-    def far_wait(side, j):
-        for c in range(pieces):
-            remote(
-                relay_out.at[side, 1, :, columns(c)],
-                far_in.at[side, j, :, columns(c)],
-                relay_send.at[side * half + 1, c],
-                relay_recv.at[side * quarter + j, c],
-                at_step(1),
-            ).wait_recv()
+    def near_send():
+        for step in range(1, quarter):
+            give_back(step).start()
+
+    def middle_send_all():
+        relay_back[2, 0] = near_out[quarter]
+        for j in range(1, quarter):
+            middle(j).start()
+
+    def near_sideways():
+        for c in range(cuts):
+            straight(c).start()
+            for j in range(1, quarter):
+                sideways(2, j, c).start()
+
+    def pass_up(side):
+        for c in range(cuts):
+            with jax.named_scope("up_" + str(c)):
+                gathered = around.at[side, pl.ds(1, quarter - 1), :, cut_columns(c)]
+                landed(gathered, side_recv.at[side, c])
+                for j in range(1, quarter):
+                    upward(side, j, c).start()
 
     def far(side):
-        pl.when(inner == 0)(lambda: far_wait(side, 0))
-        for j in range(1, quarter):
-            far_wait(side, j)
+        on_outer(lambda: landed(far_in.at[side], relay_recv.at[side]))
+        on_inner(lambda: landed(far_in.at[side, pl.ds(1, quarter - 1)], relay_recv.at[side]))
         block = far_in[side].reshape(quarter * capacity, width)
         out = gated_sum(block, gate_all, up_all, down_all).astype(jnp.bfloat16)
-        for j in range(quarter - 1, -1, -1):
-            part = out[j * capacity : (j + 1) * capacity]
-            far_out[side, j] = part
-            if j == 0:
-
-                @pl.when(inner == 0)
-                def _():
-                    home(side, 0).start()
-
-                @pl.when(inner == 1)
-                def _():
-                    relay_back[side, 0] = far_out[side, 0]
-            else:
-                home(side, j).start()
-
-    def send_sums(side):
-        places, scales = slot_places(meta_in[side], me, capacity)
-        pair = weight_matrix(places, scales, 0, half * capacity)
-        for k in range(1, half):
-            remote(
-                far_out.at[side, 1],
-                relay_back.at[side, k],
-                home_send.at[side * quarter + 1],
-                home_recv.at[side * half + k],
-                at_step(k),
-            ).wait_recv()
-        for c in range(pieces):
-            block = relay_back[side, :, :, columns(c)]
-            sums_out[side, :, columns(c)] = weighted(
-                pair, block.reshape(half * capacity, piece)
-            ).astype(jnp.bfloat16)
-            sums(side, c).start()
+        far_out[side] = out.reshape(quarter, capacity, width)
+
+        @pl.when(inner == 1)
+        def _():
+            relay_back[side, 0] = far_out[side, 0]
+            for c in range(cuts):
+                for j in range(quarter - 1, 0, -1):
+                    home(side, j, c).start()
+
+        @pl.when(inner == 0)
+        def _():
+            for c in range(cuts):
+                for j in range(1, quarter):
+                    sideways(side, j, c).start()
+                home(side, 0, c).start()
+
+    def prepare(side, source, reach):
+        places, scales = slot_places(source[...], me, capacity)
+        upper, lower = weight_matrix(places, scales, 0, reach * capacity)
+        scales_of[side, 0, :, : reach * capacity] = upper
+        scales_of[side, 1, :, : reach * capacity] = lower
+
+    def weighted_by(side, reach, block):
+        span = reach * capacity
+        pair = (scales_of[side, 0, :, :span], scales_of[side, 1, :, :span])
+        return weighted(pair, block.reshape(span, block.shape[-1]))
+
+    def send_sums(side, c):
+        landed(relay_back.at[side, pl.ds(1, half - 1), :, cut_columns(c)], home_recv.at[side, c])
+        block = relay_back[side, :, :, cut_columns(c)]
+        sums_out[side, :, cut_columns(c)] = weighted_by(side, half, block).astype(jnp.bfloat16)
+        sums(side, c).start()
+
+    def send_on(c):
+        if c == 0:
+            landed(relay_back.at[2, pl.ds(1, quarter - 1)], middle_recv.at[0])
+        block = relay_back[2, :quarter, :, cut_columns(c)]
+        own = weighted_by(2, quarter, block)
+        at = cut_columns(c)
+        landed(pass_in.at[:, at], pass_recv.at[c])
+        pass_out[:, at] = (own + pass_in[:, at].astype(jnp.float32)).astype(jnp.bfloat16)
+        sums_on(c).start()
 
     def shared():
         for i in range(len(sources)):
@@ -394,62 +552,80 @@
         total[...] = gated_sum(normed[...], s_gate_all, s_up_all, s_down_all)
 
     def near_total():
-        places, scales = slot_places(meta[...], me, capacity)
-        pair = weight_matrix(places, scales, 0, half * capacity)
-        for step in range(1, half):
-            give_back(step).wait_recv()
-        total[...] += weighted(pair, returned[...].reshape(half * capacity, width))
+        prepare(3, meta, half)
+        landed(returned.at[pl.ds(1, quarter - 1)], back_recv.at[0])
+        total[...] += weighted_by(3, quarter, returned[:quarter])
+
+    def outer_total():
+        span = quarter * capacity
+        landed(returned.at[pl.ds(quarter, quarter)], back_recv.at[1])
+        pair = (scales_of[3, 0, :, span:], scales_of[3, 1, :, span:])
+        total[...] += weighted(pair, returned[quarter:].reshape(span, width))
 
     actions = {
         "S": shared,
         "A": lambda: near(0),
         "B": lambda: near(1),
-        "a": lambda: near_send(0),
-        "b": lambda: near_send(1),
-        "F": lambda: far(1),
-        "G": lambda: far(0),
-        "1": lambda: pass_some(1, (0, 1)),
-        "2": lambda: pass_some(1, (2,)),
-        "3": lambda: pass_some(1, (3,)),
-        "4": lambda: pass_some(0, (0, 1)),
-        "5": lambda: pass_some(0, (2, 3)),
-        "X": lambda: on_inner(lambda: send_sums(1)),
-        "Y": lambda: on_inner(lambda: send_sums(0)),
+        "a": near_send,
+        "m": lambda: on_inner(middle_send_all),
+        "h": lambda: on_outer(near_sideways),
         "N": near_total,
+        "M": lambda: on_inner(outer_total),
+    }
+    numbered = {
+        "0": lambda c: on_inner(lambda: pass_on(0, c)),
+        "1": lambda c: on_inner(lambda: pass_on(1, c)),
+        "2": lambda c: on_inner(lambda: pass_on(2, c)),
+        "F": far,
+        "W": lambda side: on_outer(lambda: pass_up(side)),
+        "P": lambda side: on_inner(
+            lambda: prepare(side, meta_in.at[side], quarter if side == 2 else half)
+        ),
+        "V": lambda c: on_inner(lambda: send_on(c)),
+        "X": lambda c: on_inner(lambda: send_sums(1, c)),
+        "Y": lambda c: on_inner(lambda: send_sums(0, c)),
     }
     for name in ORDER:
-        actions[name]()
-
-    for c in range(pieces):
-        remote(
-            sums_out.at[0, :, columns(c)],
-            sums_in.at[:, columns(c)],
-            sums_send.at[c],
-            sums_recv.at[c],
-            gateway,
-        ).wait_recv()
-        mixed[:, columns(c)] = (
-            total[:, columns(c)] + sums_in[:, columns(c)].astype(jnp.float32)
-        ).astype(jnp.bfloat16)
-
-    meta_copy.wait_send()
-    for c in range(pieces):
-        block_copy(c).wait_send()
-    for step in range(1, half):
-        dispatch(step).wait_send()
-        give_back(step).wait_send()
-    for side in range(2):
-        pl.when(inner == 0)(lambda: home(side, 0).wait_send())
-        for j in range(1, quarter):
-            home(side, j).wait_send()
-
-    @pl.when(inner == 1)
-    def _():
-        for side in range(2):
-            for c in range(pieces):
-                sums(side, c).wait_send()
-                for k in range(1, half):
-                    relay(side, k, c).wait_send()
+        with jax.named_scope("do_" + name):
+            if name in actions:
+                actions[name]()
+            else:
+                numbered[name[0]](int(name[2:]))
+
+    keep = pltpu.make_async_copy(total, held, held_send.at[0])
+    keep.start()
+    with jax.named_scope("settle"):
+        left(outgoing.at[pl.ds(1, quarter - 1)], out_send.at[0])
+        left(near_out.at[pl.ds(1, quarter - 1)], back_send.at[0])
+        left(normed, block_send.at[0])
+
+        @pl.when(inner == 0)
+        def _():
+            left(meta, meta_send.at[0])
+            left(meta, meta_send.at[1])
+            left(near_out.at[quarter], up_send.at[3])
+            for side in range(2):
+                left(far_out.at[side, 0], home_send.at[side])
+            for side in range(3):
+                left(around.at[side, pl.ds(1, quarter - 1)], side_send.at[side])
+                left(around.at[side, pl.ds(1, quarter - 1)], up_send.at[side])
+
+        @pl.when(inner == 1)
+        def _():
+            left(meta, meta_send.at[0])
+            left(outgoing.at[pl.ds(quarter, quarter)], out_send.at[1])
+            left(near_out.at[pl.ds(1, quarter - 1)], middle_send.at[0])
+            left(normed, block_send.at[1])
+            for side in range(2):
+                left(far_out.at[side, pl.ds(1, quarter - 1)], home_send.at[side])
+                left(relay_out.at[side, pl.ds(1, half - 1)], relay_send.at[side])
+                left(normed, sums_send.at[side])
+            left(relay_out.at[2, pl.ds(1, quarter - 1)], relay_send.at[2])
+            left(normed, pass_send.at[0])
+
+        keep.wait()
+        for c in range(cuts):
+            landed(sums_in.at[:, cut_columns(c)], sums_recv.at[c])
 
 
 def kernel_body(
@@ -468,7 +644,7 @@
     halves = lax.axis_size("tp")
     tok_rows, width = tokens.shape
     capacity = 3 * tok_rows * expert_ids.shape[1] // (2 * peers)
-    half, quarter, pieces = peers // 2, peers // 4, 4
+    half, quarter, pieces, cuts, bands = peers // 2, peers // 4, PIECES, CUTS, 4
     vmem = pl.BlockSpec(memory_space=pltpu.VMEM)
     anywhere = pl.BlockSpec(memory_space=pl.ANY)
     weights = (
@@ -479,23 +655,24 @@
         shared_up,
         shared_down,
     )
-    meta = jnp.concatenate(
-        [expert_ids.astype(jnp.float32), route_weights, jnp.zeros((tok_rows, 4), jnp.float32)],
-        axis=1,
-    ).T
 
     def rows(*shape):
         return pltpu.VMEM(shape, jnp.bfloat16)
 
     dma = pltpu.SemaphoreType.DMA
-    return pl.pallas_call(
-        functools.partial(layer_kernel, peers, capacity, pieces),
-        out_shape=jax.ShapeDtypeStruct((tok_rows, width), jnp.bfloat16),
-        in_specs=[vmem] * 3 + [anywhere] * 6,
-        out_specs=vmem,
+    held, arrived = pl.pallas_call(
+        functools.partial(layer_kernel, peers, capacity, pieces, cuts),
+        out_shape=[
+            jax.ShapeDtypeStruct((tok_rows, width), jnp.float32),
+            jax.ShapeDtypeStruct((tok_rows, width), jnp.bfloat16),
+        ],
+        in_specs=[anywhere] + [vmem] * 3 + [anywhere] * 6,
+        out_specs=[anywhere] * 2,
         scratch_shapes=[pltpu.VMEM((halves,) + w.shape, w.dtype) for w in weights]
         + [
             rows(tok_rows, width),
+            rows(tok_rows, width),
+            pltpu.VMEM((8, tok_rows), jnp.float32),
             rows(half, capacity, width),
             rows(half, capacity, width),
             rows(2, quarter, capacity, width),
@@ -503,25 +680,30 @@
             rows(2, quarter, capacity, width),
             rows(half, capacity, width),
             pltpu.VMEM((tok_rows, width), jnp.float32),
-            rows(2, tok_rows, width),
-            pltpu.VMEM((2,) + meta.shape, jnp.float32),
-            rows(2, half * capacity, tok_rows),
-            rows(2, half, capacity, width),
-            rows(2, half, capacity, width),
+            rows(3, tok_rows, width),
+            pltpu.VMEM((3, 8, tok_rows), jnp.float32),
+            rows(3, half * capacity, tok_rows),
+            rows(4, 2, tok_rows, half * capacity),
+            rows(3, half, capacity, width),
+            rows(3, half, capacity, width),
             rows(2, tok_rows, width),
             rows(tok_rows, width),
+            rows(tok_rows, width),
+            rows(3, quarter, capacity, width),
         ]
+        + [dma((bands,))]
         + [dma((len(weights),))] * 3
-        + [dma((half,))] * 4
-        + [dma((pieces,)), dma((2, pieces)), dma((1,)), dma((2,))]
-        + [dma((2 * half, pieces)), dma((2 * quarter, pieces))]
-        + [dma((2 * quarter,)), dma((2 * half,))]
-        + [dma((2 * pieces,)), dma((pieces,))],
+        + [dma((2,)), dma((2,)), dma((1,)), dma((2,))]
+        + [dma((2,)), dma((3, pieces)), dma((2,)), dma((3,))]
+        + [dma((3,)), dma((3,)), dma((2,)), dma((2, cuts))]
+        + [dma((2,)), dma((cuts,)), dma((1,)), dma((cuts,)), dma((1,)), dma((1,))]
+        + [dma((3,)), dma((3, cuts)), dma((4,)), dma((1,))],
         compiler_params=pltpu.CompilerParams(
-            collective_id=0, has_side_effects=True, vmem_limit_bytes=60 * 1024 * 1024
+            collective_id=0, has_side_effects=True, vmem_limit_bytes=VMEM_MIB * 1024 * 1024
         ),
         name="layer",
-    )(tokens, norm_gain.reshape(1, width), meta, *weights)
+    )(tokens, norm_gain.reshape(1, width), expert_ids.T, route_weights.T, *weights)
+    return (held + arrived.astype(jnp.float32)).astype(jnp.bfloat16)
 
 
 def normalize(tokens, norm_gain):

time: 144 us -> 104 us (0.72)
  the two profiles are of different devices: /device:TPU:0 before, /device:TPU:9 now
where the time goes in v2:
time: 104 us; the launch traced here: 102 us
  Pallas kernels  98.8 us (95%)
  other arithmetic  3.11 us (3%)
    pallas_call x1, Pallas kernels, kernel_body(): pl.pallas_call(functools.partial(layer_kernel, peers, capacity, pieces, c...  98.8 us
    convert_element_type x1, other arithmetic, kernel_body(): return (held + arrived.astype(jnp.float32)).astype(jnp.bfloat16)  3.11 us

profile of v2, /device:TPU:9, one launch (start us, length us, event | category | flops | bytes accessed | tf_op | source)
XLA Modules:
  0.0 102.0 jit_solution(925203066486283773)
XLA Ops:
  0.0 98.8 %layer.1 = (f32[256,2048]{1,0:T(8,128)}, bf16[256,2048]{1,0:T(8,128)(2,1)}) custom-call(bf16[256,2048]{1,0:T(8,128)(2,1)} %tokens.1, f32[1,2048]{1,0:T(1,128)} %bitcast.9, s32[2,256]{1,0:T(2,128)} %bitcast.10, f32[2,256]{1,0:T(2,128)} %bitcast.11, bf16[2048,256]{1,0:T(8,128)(2,1)} %bitcast.6, bf16[2048,256]{1,0:T(8,128)(2,1)} %bitcast.7, ...), custom_call_target="tpu_custom_call" | custom-call | tf_op jit(solution)/shard_map/layer/pallas_call | solution.py:663
  98.9 3.1 %add_convert_fusion = bf16[256,2048]{1,0:T(8,128)(2,1)} fusion(f32[256,2048]{1,0:T(8,128)} %get-tuple-element.7, bf16[256,2048]{1,0:T(8,128)(2,1)} %get-tuple-element.8), kind=kLoop, calls=%fused_computation | loop fusion | flops 1572864 | bytes 4194304 | tf_op jit(solution)/shard_map/convert_element_type | solution.py:706

commit v3 on v2

--- a/solution.py
+++ b/solution.py
@@ -95,13 +95,14 @@
 PIECES = 8
 VMEM_MIB = 60
 CUTS = 8
-OWN_FIRST = 2
+OWN_FIRST = (2, 2)
 ORDER = (
-    "2.0", "2.1", "2.2", "2.3", "0.0", "0.1", "S", "2.4", "2.5", "0.2", "0.3", "2.6", "2.7", "A",
-    "0.4", "0.5", "B", "0.6", "0.7", "1.0", "1.1", "F.0", "W.0", "P.0", "1.2", "1.3", "P.2", "1.4",
-    "1.5", "m", "Y.0", "Y.1", "1.6", "1.7", "Y.2", "Y.3", "F.1", "W.1", "a", "h", "W.2", "Y.4",
-    "Y.5", "Y.6", "Y.7", "P.1", "V.0", "V.1", "V.2", "V.3", "V.4", "V.5", "X.0", "X.1", "X.2",
-    "X.3", "V.6", "V.7", "X.4", "X.5", "X.6", "X.7", "N", "M",
+    "2.0", "2.1", "2.2", "2.3", "0.0", "0.1", "2.4", "2.5", "0.2", "0.3", "2.6", "2.7", "Q", "O.1",
+    "0.4", "0.5", "S", "0.6", "0.7", "3.0", "3.1", "3.2", "3.3", "F.0", "W.0", "O.0", "3.4", "3.5",
+    "A", "B", "P.0", "4.0", "4.1", "P.2", "m", "4.2", "4.3", "h", "3.6", "3.7", "4.4", "4.5",
+    "Y.0", "Y.1", "4.6", "4.7", "Y.2", "Y.3", "Y.4", "Y.5", "Y.6", "Y.7", "F.1", "W.1", "W.2", "a",
+    "P.1", "V.0", "V.1", "V.2", "V.3", "V.4", "V.5", "X.0", "X.1", "X.2", "X.3", "V.6", "V.7",
+    "X.4", "X.5", "X.6", "X.7", "N", "M",
 )
 
 
@@ -174,6 +175,7 @@
     side_recv,
     up_send,
     held_send,
+    turn,
 ):
     me = lax.axis_index("ep")
     core = lax.axis_index("tp")
@@ -386,21 +388,31 @@
             at_step(next_turn),
         )
 
+    def start_own(which, first, last):
+        if last > first:
+
+            @pl.when(core == which)
+            def _():
+                for c in range(first, last):
+                    block_copy(1, c).start()
+
+    def start_block():
+        for c in range(pieces):
+            block_copy(2, c).start()
+
     with jax.named_scope("meet"):
         pl.semaphore_wait(barrier, len(greeted) + 1)
 
     @pl.when(inner == 1)
     def _():
         meta_copy(1).start()
-        for c in range(OWN_FIRST):
-            block_copy(1, c).start()
+        start_own(1, 0, OWN_FIRST[1])
 
     @pl.when(inner == 0)
     def _():
         meta_copy(2).start()
         meta_copy(0).start()
-        for c in range(pieces):
-            block_copy(2, c).start()
+        pl.when(core == 0)(start_block)
 
     for copy in local:
         copy.start()
@@ -425,6 +437,16 @@
     for copy in swaps:
         copy.start()
 
+    @pl.when((inner == 0) & (core == 0))
+    def _():
+        left(normed, block_send.at[0])
+        pl.semaphore_signal(turn, inc=1, device_id=(me, sibling), device_id_type=MESH)
+
+    @pl.when((inner == 0) & (core == 1))
+    def _():
+        pl.semaphore_wait(turn, 1)
+        start_block()
+
     def open_side(side):
         landed(meta_in.at[side], meta_recv.at[side])
         reach = quarter if side == 2 else half
@@ -439,9 +461,6 @@
         landed(relay_in.at[side, :, columns(c)], block_recv.at[side, c])
         if side == 2:
             forward(c).start()
-            if c == pieces - 1:
-                for own in range(OWN_FIRST, pieces):
-                    block_copy(1, own).start()
         rows = jnp.dot(
             picked[side, : reach * capacity],
             relay_in[side, :, columns(c)],
@@ -570,12 +589,16 @@
         "m": lambda: on_inner(middle_send_all),
         "h": lambda: on_outer(near_sideways),
         "N": near_total,
+        "Q": lambda: on_inner(lambda: start_own(0, 0, OWN_FIRST[0])),
         "M": lambda: on_inner(outer_total),
     }
     numbered = {
         "0": lambda c: on_inner(lambda: pass_on(0, c)),
         "1": lambda c: on_inner(lambda: pass_on(1, c)),
         "2": lambda c: on_inner(lambda: pass_on(2, c)),
+        "3": lambda c: pl.when((inner == 1) & (core == 1))(lambda: pass_on(1, c)),
+        "4": lambda c: pl.when((inner == 1) & (core == 0))(lambda: pass_on(1, c)),
+        "O": lambda which: on_inner(lambda: start_own(which, OWN_FIRST[which], pieces)),
         "F": far,
         "W": lambda side: on_outer(lambda: pass_up(side)),
         "P": lambda side: on_inner(
@@ -597,7 +620,10 @@
     with jax.named_scope("settle"):
         left(outgoing.at[pl.ds(1, quarter - 1)], out_send.at[0])
         left(near_out.at[pl.ds(1, quarter - 1)], back_send.at[0])
-        left(normed, block_send.at[0])
+
+        @pl.when((inner == 1) | (core == 1))
+        def _():
+            left(normed, block_send.at[0])
 
         @pl.when(inner == 0)
         def _():
@@ -697,7 +723,8 @@
         + [dma((2,)), dma((3, pieces)), dma((2,)), dma((3,))]
         + [dma((3,)), dma((3,)), dma((2,)), dma((2, cuts))]
         + [dma((2,)), dma((cuts,)), dma((1,)), dma((cuts,)), dma((1,)), dma((1,))]
-        + [dma((3,)), dma((3, cuts)), dma((4,)), dma((1,))],
+        + [dma((3,)), dma((3, cuts)), dma((4,)), dma((1,))]
+        + [pltpu.SemaphoreType.REGULAR],
         compiler_params=pltpu.CompilerParams(
             collective_id=0, has_side_effects=True, vmem_limit_bytes=VMEM_MIB * 1024 * 1024
         ),

time: 104 us -> 103 us (level); the launches traced: 102 us -> 102 us
  no operation moved by 1% of the time
where the time goes in v3:
time: 103 us; the launch traced here: 102 us
  Pallas kernels  99.4 us (97%)
  other arithmetic  3.11 us (3%)
    pallas_call x1, Pallas kernels, kernel_body(): pl.pallas_call(functools.partial(layer_kernel, peers, capacity, pieces, c...  99.4 us
    convert_element_type x1, other arithmetic, kernel_body(): return (held + arrived.astype(jnp.float32)).astype(jnp.bfloat16)  3.11 us

profile of v3, /device:TPU:9, one launch (start us, length us, event | category | flops | bytes accessed | tf_op | source)
XLA Modules:
  0.0 102.5 jit_solution(5062616367101931303)
XLA Ops:
  0.0 99.4 %layer.1 = (f32[256,2048]{1,0:T(8,128)}, bf16[256,2048]{1,0:T(8,128)(2,1)}) custom-call(bf16[256,2048]{1,0:T(8,128)(2,1)} %tokens.1, f32[1,2048]{1,0:T(1,128)} %bitcast.9, s32[2,256]{1,0:T(2,128)} %bitcast.10, f32[2,256]{1,0:T(2,128)} %bitcast.11, bf16[2048,256]{1,0:T(8,128)(2,1)} %bitcast.6, bf16[2048,256]{1,0:T(8,128)(2,1)} %bitcast.7, ...), custom_call_target="tpu_custom_call" | custom-call | tf_op jit(solution)/shard_map/layer/pallas_call | solution.py:689
  99.4 3.1 %add_convert_fusion = bf16[256,2048]{1,0:T(8,128)(2,1)} fusion(f32[256,2048]{1,0:T(8,128)} %get-tuple-element.7, bf16[256,2048]{1,0:T(8,128)(2,1)} %get-tuple-element.8), kind=kLoop, calls=%fused_computation | loop fusion | flops 1572864 | bytes 4194304 | tf_op jit(solution)/shard_map/convert_element_type | solution.py:733

commit v4 on v3

--- a/solution.py
+++ b/solution.py
@@ -98,8 +98,8 @@
 OWN_FIRST = (2, 2)
 ORDER = (
     "2.0", "2.1", "2.2", "2.3", "0.0", "0.1", "2.4", "2.5", "0.2", "0.3", "2.6", "2.7", "Q", "O.1",
-    "0.4", "0.5", "S", "0.6", "0.7", "3.0", "3.1", "3.2", "3.3", "F.0", "W.0", "O.0", "3.4", "3.5",
-    "A", "B", "P.0", "4.0", "4.1", "P.2", "m", "4.2", "4.3", "h", "3.6", "3.7", "4.4", "4.5",
+    "0.4", "0.5", "S", "0.6", "0.7", "3.0", "3.1", "3.2", "3.3", "F.0", "O.0", "3.4", "3.5", "A",
+    "B", "W.0", "h", "P.0", "4.0", "4.1", "P.2", "m", "4.2", "4.3", "3.6", "3.7", "4.4", "4.5",
     "Y.0", "Y.1", "4.6", "4.7", "Y.2", "Y.3", "Y.4", "Y.5", "Y.6", "Y.7", "F.1", "W.1", "W.2", "a",
     "P.1", "V.0", "V.1", "V.2", "V.3", "V.4", "V.5", "X.0", "X.1", "X.2", "X.3", "V.6", "V.7",
     "X.4", "X.5", "X.6", "X.7", "N", "M",

time: 103 us -> 103 us (level)
  no operation moved by 1% of the time
where the time goes in v4:
time: 103 us; the launch traced here: 102 us
  Pallas kernels  99.4 us (97%)
  other arithmetic  3.11 us (3%)
    pallas_call x1, Pallas kernels, kernel_body(): pl.pallas_call(functools.partial(layer_kernel, peers, capacity, pieces, c...  99.4 us
    convert_element_type x1, other arithmetic, kernel_body(): return (held + arrived.astype(jnp.float32)).astype(jnp.bfloat16)  3.11 us

profile of v4, /device:TPU:9, one launch (start us, length us, event | category | flops | bytes accessed | tf_op | source)
XLA Modules:
  0.0 102.5 jit_solution(534268964642941321)
XLA Ops:
  0.0 99.4 %layer.1 = (f32[256,2048]{1,0:T(8,128)}, bf16[256,2048]{1,0:T(8,128)(2,1)}) custom-call(bf16[256,2048]{1,0:T(8,128)(2,1)} %tokens.1, f32[1,2048]{1,0:T(1,128)} %bitcast.9, s32[2,256]{1,0:T(2,128)} %bitcast.10, f32[2,256]{1,0:T(2,128)} %bitcast.11, bf16[2048,256]{1,0:T(8,128)(2,1)} %bitcast.6, bf16[2048,256]{1,0:T(8,128)(2,1)} %bitcast.7, ...), custom_call_target="tpu_custom_call" | custom-call | tf_op jit(solution)/shard_map/layer/pallas_call | solution.py:689
  99.4 3.1 %add_convert_fusion = bf16[256,2048]{1,0:T(8,128)(2,1)} fusion(f32[256,2048]{1,0:T(8,128)} %get-tuple-element.7, bf16[256,2048]{1,0:T(8,128)(2,1)} %get-tuple-element.8), kind=kLoop, calls=%fused_computation | loop fusion | flops 1572864 | bytes 4194304 | tf_op jit(solution)/shard_map/convert_element_type | solution.py:733
